TPU v7x, 32 devices: a whole 2x2x4 slice. The times are simulated.
32 devices in a mesh: sp: 8 (over z, y), tp: 4 (over x, core).
Axes of the slice: x: 2, y: 2, z: 4, core: 2. Of those that a mesh axis runs over, the one named last changes fastest.
Arguments:
- residual: bfloat16 [6144, 2048], P(('sp', 'tp')), may hold values from -6 to 6
- queries: bfloat16 [6144, 1024], P('sp', 'tp'), may hold values from -240 to 240
- keys: bfloat16 [6144, 256], P('sp', 'tp'), may hold values from -6 to 6
- values: bfloat16 [6144, 256], P('sp', 'tp'), may hold values from -18 to 18
- sinks: float32 [16], P('tp'), may hold values from 1 to 6
- out_weight: bfloat16 [1024, 2048], replicated, may hold values from -0.5625 to 0.5625
- norm_gain: float32 [2048], replicated, may hold values from 0.1 to 1.9
- gate_weight: bfloat16 [2048, 5632], P('sp', 'tp'), may hold values from -0.125 to 0.125
- up_weight: bfloat16 [2048, 5632], P('sp', 'tp'), may hold values from -0.125 to 0.125
- down_weight: bfloat16 [5632, 2048], P('tp', 'sp'), may hold values from -0.078125 to 0.078125
Outputs:
- layer_out: bfloat16 [6144, 2048], P(('sp', 'tp'))
All inputs are finite; a program needn't handle non-finite values.
Results may differ from a plain program's by a relative error of at most 0.014.
Values may be sent and summed in bfloat16 or wider, within the bound.
No kernel may reach another device: no remote copies, remote signals or barrier semaphores. Data moves between devices by JAX's collectives and lax.ppermute only.
A program may use at most 128 MiB of HBM per device.

v0:
```python
import jax
import jax.numpy as jnp
from jax import lax
from jax.sharding import PartitionSpec as P

HEAD = 64
WINDOW = 128


def passed_along(block, axis, distance):
    devices = range(lax.axis_size(axis))
    route = [(i - distance, i) for i in devices if i - distance in devices]
    return lax.ppermute(block, axis, route)


def attend(queries, keys_ext, values_ext, sinks, block_base):
    rows = queries.shape[0]
    nblk = rows // WINDOW
    qheads = sinks.shape[0]
    kheads = keys_ext.shape[1] // HEAD
    group = qheads // kheads
    qblock = queries.reshape(nblk, WINDOW, kheads, group, HEAD).astype(jnp.float32)

    def band(arr):
        first = arr[:rows].reshape(nblk, WINDOW, kheads, HEAD)
        second = arr[WINDOW:].reshape(nblk, WINDOW, kheads, HEAD)
        return jnp.concatenate([first, second], axis=1).astype(jnp.float32)

    kband = band(keys_ext)
    vband = band(values_ext)
    score = jnp.einsum("nqhgd,nkhd->nhgqk", qblock, kband) * HEAD ** (-0.5)
    qidx = jnp.arange(WINDOW)[:, None]
    kidx = jnp.arange(2 * WINDOW)[None, :]
    rel = qidx + WINDOW - kidx
    valid = (rel >= 0) & (rel < WINDOW)
    blocks = block_base + jnp.arange(nblk)
    valid = valid[None] & ((blocks > 0)[:, None, None] | (kidx >= WINDOW)[None])
    score = jnp.where(valid[:, None, None], score, -jnp.inf)
    sink = sinks.reshape(kheads, group)[None, :, :, None]
    top = jnp.maximum(jnp.max(score, axis=-1), sink)
    expd = jnp.exp(score - top[..., None])
    denom = jnp.sum(expd, axis=-1) + jnp.exp(sink - top)
    weights = (expd / denom[..., None]).astype(jnp.bfloat16)
    result = jnp.einsum("nhgqk,nkhd->nqhgd", weights.astype(jnp.float32), vband)
    return result.reshape(rows, qheads * HEAD).astype(jnp.bfloat16)


def shards(
    residual,
    queries,
    keys,
    values,
    sinks,
    out_weight,
    norm_gain,
    gate_weight,
    up_weight,
    down_weight,
):
    rows_dev = queries.shape[0]
    prev_keys, prev_values = passed_along((keys[-WINDOW:], values[-WINDOW:]), "sp", 1)
    keys_ext = jnp.concatenate([prev_keys, keys], axis=0)
    values_ext = jnp.concatenate([prev_values, values], axis=0)
    attention = attend(
        queries, keys_ext, values_ext, sinks, lax.axis_index("sp") * (rows_dev // WINDOW)
    )
    width = attention.shape[1]
    mine = lax.dynamic_slice_in_dim(out_weight, lax.axis_index("tp") * width, width, 0)
    proj = lax.psum_scatter(
        jnp.dot(attention, mine, preferred_element_type=jnp.float32).astype(jnp.bfloat16),
        "tp",
        scatter_dimension=0,
        tiled=True,
    ).astype(jnp.float32)
    mixed = (residual.astype(jnp.float32) + proj).astype(jnp.bfloat16)
    mixf = mixed.astype(jnp.float32)
    normed = (
        mixf * lax.rsqrt(jnp.mean(mixf * mixf, axis=-1, keepdims=True) + 1e-06) * norm_gain
    ).astype(jnp.bfloat16)
    normed_all = lax.all_gather(normed, "tp", axis=0, tiled=True)
    gate = jnp.dot(
        normed_all,
        lax.all_gather(gate_weight, "sp", axis=0, tiled=True),
        preferred_element_type=jnp.float32,
    )
    upper = jnp.dot(
        normed_all,
        lax.all_gather(up_weight, "sp", axis=0, tiled=True),
        preferred_element_type=jnp.float32,
    )
    hidden = (jax.nn.silu(gate) * upper).astype(jnp.bfloat16)
    terms = jnp.dot(
        hidden,
        lax.all_gather(down_weight, "sp", axis=1, tiled=True),
        preferred_element_type=jnp.float32,
    )
    ffn = lax.psum_scatter(
        terms.astype(jnp.bfloat16), "tp", scatter_dimension=0, tiled=True
    ).astype(jnp.float32)
    return (mixed.astype(jnp.float32) + ffn).astype(jnp.bfloat16)


def solution(mesh):
    placed = (
        P(("sp", "tp"), None),
        P("sp", "tp"),
        P("sp", "tp"),
        P("sp", "tp"),
        P("tp"),
        P(),
        P(),
        P("sp", "tp"),
        P("sp", "tp"),
        P("tp", "sp"),
    )
    return jax.shard_map(
        shards, mesh=mesh, in_specs=placed, out_specs=P(("sp", "tp"), None), check_vma=False
    )
```

profile of v0, /device:TPU:0, one launch (start us, length us, event | category | flops | bytes accessed | tf_op | source)
XLA Modules:
  0.0 407.9 jit_solution(3157988359120101178)
XLA Ops:
  7.4 0.0 reduce-scatter.3.cloned.1.call-start
  7.4 0.7 slice.14
  8.1 4.9 %collective-permute-start.1 = (bf16[128,64]{0,1:T(8,128)(2,1)S(1)}, bf16[128,64]{0,1:T(8,128)(2,1)S(1)}, u32[]{:S(2)}, u32[]{:S(2)}) collective-permute-start(bf16[128,64]{0,1:T(8,128)(2,1)S(1)} %slice.14), channel_id=1, source_target_pairs={{0,4},{4,8},{8,12},{12,16},{16,20},{20,24},{24,28},{1,5},{5,9},{9,... | collective-permute-start | bytes 49160 | tf_op jit(solution)/shard_map/ppermute | solution.py:13
  13.0 0.7 slice.12
  13.7 3.4 collective-permute-start
  17.2 0.1 broadcast_or_fusion
  17.3 0.3 broadcast_and_fusion
  17.6 1.0 reshape.145
  18.6 1.0 reshape.142
  19.6 0.0 copy-start.4
  19.6 2.5 reshape.151
  22.2 0.6 copy.14
  22.9 0.0 collective-permute-done.1
  22.9 0.9 pad_maximum_fusion
  23.8 0.1 reshape.144
  23.9 0.0 copy-start.2
  23.9 1.9 fusion.1
  25.8 0.0 copy-done.4
  25.8 0.1 broadcast_maximum_fusion
  25.9 0.7 fusion
  26.6 0.1 exponential_add_fusion
  26.7 0.0 collective-permute-done
  26.7 0.0 copy-done.2
  26.7 0.7 pad_maximum_fusion.1
  27.3 1.0 reshape.141
  28.4 1.8 fusion.12
  30.2 0.3 copy.20
  30.5 4.0 convolution_convert_fusion
  34.5 0.0 copy-start
  34.5 0.0 copy-start.3
  34.5 0.0 reduce-scatter.3.cloned.1.call-update
  34.5 0.0 all-gather.7.cloned.1.call-start
  34.6 0.5 all-gather.7.cloned.1.call-update
  35.1 0.0 all-gather.5.cloned.1.call-start
  35.1 37.7 %reduce-scatter.3.cloned.1.call-done = bf16[192,2048]{1,0:T(8,128)(2,1)} async-done(((bf16[768,2048]{1,0:T(8,128)(2,1)}), bf16[192,2048]{1,0:T(8,128)(2,1)}) %reduce-scatter.3.cloned.1.call-update) | async-done | bytes 786448 | tf_op jit(solution)/shard_map/reduce_scatter | solution.py:69
  72.8 0.0 copy-done
  72.8 1.5 fusion.2
  74.3 0.0 copy-done.3
  74.3 2.3 fusion.4
  76.6 0.0 all-gather.5.cloned.1.call-update
  76.6 0.0 all-gather.11.cloned.1.call-start
  76.7 0.5 all-gather.11.cloned.1.call-update
  77.2 0.0 all-gather.9.cloned.1.call-start
  77.3 0.7 all-gather.9.cloned.1.call-update
  77.9 0.2 reduce-scatter.5.cloned.1.call-start
  78.2 51.4 %all-gather.7.cloned.1.call-done = bf16[2048,1408]{1,0:T(8,128)(2,1)} async-done(((bf16[256,1408]{1,0:T(8,128)(2,1)}), bf16[2048,1408]{1,0:T(8,128)(2,1)}) %all-gather.7.cloned.1.call-update) | async-done | bytes 5767184 | tf_op jit(solution)/shard_map/all_gather | solution.py:83
  129.6 28.0 %all-gather.5.cloned.1.call-done = bf16[768,2048]{1,0:T(8,128)(2,1)} async-done(((bf16[192,2048]{1,0:T(8,128)(2,1)}), bf16[768,2048]{1,0:T(8,128)(2,1)}) %all-gather.5.cloned.1.call-update) | async-done | bytes 3145744 | tf_op jit(solution)/shard_map/all_gather | solution.py:80
  157.6 9.7 %fusion.33 = f32[768,1408]{1,0:T(8,128)} fusion(bf16[768,2048]{1,0:T(8,128)(2,1)} %all-gather.5.cloned.1.call-done, bf16[2048,1408]{1,0:T(8,128)(2,1)} %all-gather.7.cloned.1.call-done), kind=kOutput, calls=%fused_computation.52 | convolution fusion | flops 4429185024 | bytes 13238272 | tf_op jit(solution)/shard_map/dot_general | solution.py:81
  167.2 85.1 %all-gather.11.cloned.1.call-done = bf16[1408,2048]{1,0:T(8,128)(2,1)} async-done(((bf16[1408,256]{1,0:T(8,128)(2,1)}), bf16[1408,2048]{1,0:T(8,128)(2,1)}) %all-gather.11.cloned.1.call-update) | async-done | bytes 5767184 | tf_op jit(solution)/shard_map/all_gather | solution.py:94
  252.4 92.5 %all-gather.9.cloned.1.call-done = bf16[2048,1408]{1,0:T(8,128)(2,1)} async-done(((bf16[256,1408]{1,0:T(8,128)(2,1)}), bf16[2048,1408]{1,0:T(8,128)(2,1)}) %all-gather.9.cloned.1.call-update) | async-done | bytes 5767184 | tf_op jit(solution)/shard_map/all_gather | solution.py:88
  344.9 16.8 %convolution_convert_fusion.1 = bf16[768,2048]{1,0:T(8,128)(2,1)} fusion(bf16[1408,2048]{1,0:T(8,128)(2,1)} %all-gather.11.cloned.1.call-done, f32[768,1408]{1,0:T(8,128)} %fusion.33, bf16[768,2048]{1,0:T(8,128)(2,1)} %all-gather.5.cloned.1.call-done, bf16[2048,1408]{1,0:T(8,128)(2,1)} %all-gather.9.cloned.1.call-done), kind=kOutput, calls=%fused_computation.2 | convolution fusion | flops 8866430976 | bytes 22151168 | tf_op jit(solution)/shard_map/dot_general | solution.py:92
  361.7 0.0 copy-start.1
  361.7 0.0 reduce-scatter.5.cloned.1.call-update
  361.7 36.2 %reduce-scatter.5.cloned.1.call-done = bf16[192,2048]{1,0:T(8,128)(2,1)} async-done(((bf16[768,2048]{1,0:T(8,128)(2,1)}), bf16[192,2048]{1,0:T(8,128)(2,1)}) %reduce-scatter.5.cloned.1.call-update) | async-done | bytes 786448 | tf_op jit(solution)/shard_map/reduce_scatter | solution.py:97
  397.9 0.0 copy-done.1
  397.9 2.4 fusion.5
  (8 shorter events, 0.1 us)
Async XLA Ops:
  7.4 65.4 %reduce-scatter.3.cloned.1.call-start = ((), (), s32[]{:S(2)}) async-start(), calls=%async_computation.2 | async-start | bytes 3932160 | tf_op jit(solution)/shard_map/reduce_scatter | solution.py:69
  8.1 14.8 %collective-permute-start.1 = (bf16[128,64]{0,1:T(8,128)(2,1)S(1)}, bf16[128,64]{0,1:T(8,128)(2,1)S(1)}, u32[]{:S(2)}, u32[]{:S(2)}) collective-permute-start(bf16[128,64]{0,1:T(8,128)(2,1)S(1)} %slice.14), channel_id=1, source_target_pairs={{0,4},{4,8},{8,12},{12,16},{16,20},{20,24},{24,28},{1,5},{5,9},{9,... | collective-permute-start | bytes 49160 | tf_op jit(solution)/shard_map/ppermute | solution.py:13
  13.7 13.0 %collective-permute-start = (bf16[128,64]{0,1:T(8,128)(2,1)S(1)}, bf16[128,64]{0,1:T(8,128)(2,1)S(1)}, u32[]{:S(2)}, u32[]{:S(2)}) collective-permute-start(bf16[128,64]{0,1:T(8,128)(2,1)S(1)} %slice.12), channel_id=1, source_target_pairs={{0,4},{4,8},{8,12},{12,16},{16,20},{20,24},{24,28},{1,5},{5,9},{9,... | collective-permute-start | bytes 49160 | tf_op jit(solution)/shard_map/ppermute | solution.py:13
  19.6 6.2 %copy-start.4 = (f32[4]{0:T(128)S(1)}, f32[4]{0:T(128)}, u32[]{:S(2)}) copy-start(f32[4]{0:T(128)} %param.14) | copy-start | bytes 52
  23.9 2.8 copy-start.2
  34.5 38.3 %copy-start = (bf16[192,2048]{1,0:T(8,128)(2,1)S(1)}, bf16[192,2048]{1,0:T(8,128)(2,1)}, u32[]{:S(2)}) copy-start(bf16[192,2048]{1,0:T(8,128)(2,1)} %param.10) | copy-start | bytes 2359300
  34.5 39.8 %copy-start.3 = (f32[2048]{0:T(1024)S(1)}, f32[2048]{0:T(1024)}, u32[]{:S(2)}) copy-start(f32[2048]{0:T(1024)} %param.16) | copy-start | bytes 24580
  34.5 95.1 %all-gather.7.cloned.1.call-start = ((), (), s32[]{:S(2)}) async-start(), calls=%async_computation.4 | async-start | bytes 6488064 | tf_op jit(solution)/shard_map/all_gather | solution.py:83
  35.1 122.5 %all-gather.5.cloned.1.call-start = ((), (), s32[]{:S(2)}) async-start(), calls=%async_computation.3 | async-start | bytes 3932160 | tf_op jit(solution)/shard_map/all_gather | solution.py:80
  76.6 175.8 %all-gather.11.cloned.1.call-start = ((), (), s32[]{:S(2)}) async-start(), calls=%async_computation.6 | async-start | bytes 6488064 | tf_op jit(solution)/shard_map/all_gather | solution.py:94
  77.2 267.7 %all-gather.9.cloned.1.call-start = ((), (), s32[]{:S(2)}) async-start(), calls=%async_computation.5 | async-start | bytes 6488064 | tf_op jit(solution)/shard_map/all_gather | solution.py:88
  77.9 320.0 %reduce-scatter.5.cloned.1.call-start = ((), (), s32[]{:S(2)}) async-start(), calls=%async_computation.7 | async-start | bytes 3932160 | tf_op jit(solution)/shard_map/reduce_scatter | solution.py:97
  361.7 36.2 %copy-start.1 = (bf16[192,2048]{1,0:T(8,128)(2,1)S(1)}, bf16[192,2048]{1,0:T(8,128)(2,1)}, u32[]{:S(2)}) copy-start(bf16[192,2048]{1,0:T(8,128)(2,1)} %reduce-scatter.3.cloned.1.call-done) | copy-start | bytes 2359300
Sparse Core Ops, SparseCore 0:
  34.6 38.1 reduce-scatter.2
  361.9 35.9 reduce-scatter.4
Sparse Core Ops, SparseCore 1:
  37.2 92.4 all-gather.6
  131.0 26.5 all-gather.4
  159.5 92.9 all-gather.10
  254.6 90.3 all-gather.8
where the time goes:
time: 409 us; the launch traced here: 408 us
  waiting for transfers between devices  333 us (81%)
  matrix products  34.1 us (8%)
  between operations  15.2 us (4%)
  other arithmetic  8.99 us (2%)
  starting transfers between devices  8.7 us (2%)
  local copies, waits for them, and re-layouts  8.18 us (2%)
    all_gather x1, waiting for transfers between devices, shards(): lax.all_gather(up_weight, 'sp', axis=0, tiled=True)  92.5 us
    all_gather x1, waiting for transfers between devices, shards(): lax.all_gather(down_weight, 'sp', axis=1, tiled=True)  85.1 us
    all_gather x1, waiting for transfers between devices, shards(): lax.all_gather(gate_weight, 'sp', axis=0, tiled=True)  51.4 us
    reduce_scatter x1, waiting for transfers between devices, shards(): lax.psum_scatter(jnp.dot(attention, mine, preferred_element_type=jnp.floa...  37.7 us
    reduce_scatter x1, waiting for transfers between devices, shards(): lax.psum_scatter(terms.astype(jnp.bfloat16), 'tp', scatter_dimension=0, t...  36.2 us
    all_gather x1, waiting for transfers between devices, shards(): normed_all = lax.all_gather(normed, 'tp', axis=0, tiled=True)  28 us
    dot_general x1, matrix products, shards(): jnp.dot(hidden, lax.all_gather(down_weight, 'sp', axis=1, tiled=True), pr...  16.8 us
    dot_general x1, matrix products, shards(): jnp.dot(normed_all, lax.all_gather(gate_weight, 'sp', axis=0, tiled=True)...  9.69 us
  transfers between devices with their start and end apart: 8, of which 6 were waited for; matrix products, arithmetic and copies ran while one was open for 6% of the time, Pallas kernels for 0%

commit v1 on v0

--- a/solution.py
+++ b/solution.py
@@ -77,7 +77,12 @@
     normed = (
         mixf * lax.rsqrt(jnp.mean(mixf * mixf, axis=-1, keepdims=True) + 1e-06) * norm_gain
     ).astype(jnp.bfloat16)
-    normed_all = lax.all_gather(normed, "tp", axis=0, tiled=True)
+    ring = [normed]
+    for hop in range(3):
+        ring.append(lax.ppermute(ring[-1], "tp", [(dev, (dev + 1) % 4) for dev in range(4)]))
+    normed_all = jnp.roll(
+        jnp.concatenate(ring[::-1], axis=0), (lax.axis_index("tp") + 1) * ring[0].shape[0], axis=0
+    )
     gate = jnp.dot(
         normed_all,
         lax.all_gather(gate_weight, "sp", axis=0, tiled=True),

time: 409 us -> 377 us (0.922)
  waiting for transfers between devices: 333 us -> 294 us
  local copies, waits for them, and re-layouts: 8.18 us -> 17.4 us
    all_gather x1, waiting for transfers between devices: 51.4 us -> 9.53 us  [shards(): lax.all_gather(gate_weight, 'sp', axis=0, tiled=True)]
    ppermute x0 -> x3, waiting for transfers between devices: none -> 34.3 us  [shards(): lax.ppermute(ring[-1], 'tp', [(dev, (dev + 1) % 4) for dev in range(4)])]
    all_gather x1 -> x0, waiting for transfers between devices: 28 us -> none  [shards(): normed_all = lax.all_gather(normed, 'tp', axis=0, tiled=True)]
    unnamed x10 -> x19, local copies, waits for them, and re-layouts: 0.02 us -> 10.5 us
    all_gather x1, waiting for transfers between devices: 92.5 us -> 82.7 us  [shards(): lax.all_gather(up_weight, 'sp', axis=0, tiled=True)]
    all_gather x1, waiting for transfers between devices: 85.1 us -> 93 us  [shards(): lax.all_gather(down_weight, 'sp', axis=1, tiled=True)]
  transfers between devices with their start and end apart: 8 -> 10, of which waited for: 6 -> 8; matrix products, arithmetic and copies ran while one was open for 6% -> 8% of each run, Pallas kernels for 0% -> 0%
where the time goes in v1:
time: 377 us
  waiting for transfers between devices  294 us (78%)
  matrix products  34 us (9%)
  local copies, waits for them, and re-layouts  17.4 us (5%)
  between operations  15.3 us (4%)
  starting transfers between devices  8.53 us (2%)
  other arithmetic  7.54 us (2%)
    all_gather x1, waiting for transfers between devices, shards(): lax.all_gather(down_weight, 'sp', axis=1, tiled=True)  93 us
    all_gather x1, waiting for transfers between devices, shards(): lax.all_gather(up_weight, 'sp', axis=0, tiled=True)  82.7 us
    reduce_scatter x1, waiting for transfers between devices, shards(): lax.psum_scatter(jnp.dot(attention, mine, preferred_element_type=jnp.floa...  36.5 us
    reduce_scatter x1, waiting for transfers between devices, shards(): lax.psum_scatter(terms.astype(jnp.bfloat16), 'tp', scatter_dimension=0, t...  36.2 us
    ppermute x3, waiting for transfers between devices, shards(): lax.ppermute(ring[-1], 'tp', [(dev, (dev + 1) % 4) for dev in range(4)])  34.3 us
    dot_general x1, matrix products, shards(): jnp.dot(hidden, lax.all_gather(down_weight, 'sp', axis=1, tiled=True), pr...  16.8 us
    unnamed x19, local copies, waits for them, and re-layouts  10.5 us
    dot_general x1, matrix products, shards(): jnp.dot(normed_all, lax.all_gather(gate_weight, 'sp', axis=0, tiled=True)...  9.7 us
  transfers between devices with their start and end apart: 10, of which 8 were waited for; matrix products, arithmetic and copies ran while one was open for 8% of the time, Pallas kernels for 0%

profile of v1, /device:TPU:0, one launch (start us, length us, event | category | flops | bytes accessed | tf_op | source)
XLA Modules:
  0.0 376.5 jit_solution(2537932385554947819)
XLA Ops:
  7.4 0.0 reduce-scatter.3.cloned.1.call-start
  7.4 0.7 slice.14
  8.1 4.9 %collective-permute-start.1 = (bf16[128,64]{0,1:T(8,128)(2,1)S(1)}, bf16[128,64]{0,1:T(8,128)(2,1)S(1)}, u32[]{:S(2)}, u32[]{:S(2)}) collective-permute-start(bf16[128,64]{0,1:T(8,128)(2,1)S(1)} %slice.14), channel_id=1, source_target_pairs={{0,4},{4,8},{8,12},{12,16},{16,20},{20,24},{24,28},{1,5},{5,9},{9,... | collective-permute-start | bytes 49160 | tf_op jit(solution)/shard_map/ppermute | solution.py:13
  13.0 0.7 slice.12
  13.7 3.4 collective-permute-start
  17.2 0.1 broadcast_or_fusion
  17.3 0.3 broadcast_and_fusion
  17.6 1.0 reshape.145
  18.6 1.0 reshape.142
  19.6 1.8 reshape.151
  21.5 0.0 collective-permute-done.1
  21.6 0.9 pad_maximum_fusion
  22.5 0.0 copy-start.3
  22.5 0.1 reshape.144
  22.6 0.7 fusion.7
  23.4 0.0 copy-start.2
  23.4 0.0 copy-done.5
  23.4 0.1 broadcast_maximum_fusion
  23.5 1.5 copy-done.2
  25.0 0.7 fusion
  25.7 0.1 exponential_add_fusion
  25.8 0.0 collective-permute-done
  25.8 0.0 copy-done.3
  25.8 0.1 reshape.141
  26.0 2.8 fusion.18
  28.8 0.3 copy.20
  29.1 0.0 copy-start
  29.1 4.0 %convolution_convert_fusion = bf16[768,2048]{1,0:T(8,128)(2,1)} fusion(bf16[1024,2048]{1,0:T(8,128)(2,1)} %param.15, s32[]{:T(128)S(6)} %select_n.21, bf16[32,8,6,128]{3,2,1,0:T(8,128)(2,1)S(1)} %bitcast.60), kind=kOutput, calls=%fused_computation.1 | convolution fusion | flops 806879232 | bytes 4587524 | tf_op jit(solution)/shard_map/dot_general | solution.py:70
  33.1 0.0 reduce-scatter.3.cloned.1.call-update
  33.1 0.0 all-gather.4.cloned.1.call-start
  33.2 0.5 all-gather.4.cloned.1.call-update
  33.7 0.0 all-gather.6.cloned.1.call-start
  33.7 0.5 all-gather.6.cloned.1.call-update
  34.3 0.0 all-gather.8.cloned.1.call-start
  34.3 0.5 all-gather.8.cloned.1.call-update
  34.9 0.0 reduce-scatter.5.cloned.1.call-start
  34.9 36.5 %reduce-scatter.3.cloned.1.call-done = bf16[192,2048]{1,0:T(8,128)(2,1)} async-done(((bf16[768,2048]{1,0:T(8,128)(2,1)}), bf16[192,2048]{1,0:T(8,128)(2,1)}) %reduce-scatter.3.cloned.1.call-update) | async-done | bytes 786448 | tf_op jit(solution)/shard_map/reduce_scatter | solution.py:69
  71.4 0.0 copy-done
  71.4 1.5 fusion.8
  72.9 0.0 copy-done.4
  72.9 1.5 fusion.10
  74.3 0.1 collective-permute-start.2
  74.4 11.4 %collective-permute-done.2 = bf16[192,2048]{1,0:T(8,128)(2,1)S(1)} collective-permute-done((bf16[192,2048]{1,0:T(8,128)(2,1)S(1)}, bf16[192,2048]{1,0:T(8,128)(2,1)S(1)}, u32[]{:S(2)}, u32[]{:S(2)}) %collective-permute-start.2) | collective-permute-done | bytes 786464 | tf_op jit(solution)/shard_map/ppermute | solution.py:82
  85.8 0.0 collective-permute-start.3
  85.8 11.4 %collective-permute-done.3 = bf16[192,2048]{1,0:T(8,128)(2,1)S(1)} collective-permute-done((bf16[192,2048]{1,0:T(8,128)(2,1)S(1)}, bf16[192,2048]{1,0:T(8,128)(2,1)S(1)}, u32[]{:S(2)}, u32[]{:S(2)}) %collective-permute-start.3) | collective-permute-done | bytes 786464 | tf_op jit(solution)/shard_map/ppermute | solution.py:82
  97.2 0.0 collective-permute-start.4
  97.2 11.5 %collective-permute-done.4 = bf16[192,2048]{1,0:T(8,128)(2,1)} collective-permute-done((bf16[192,2048]{1,0:T(8,128)(2,1)S(1)}, bf16[192,2048]{1,0:T(8,128)(2,1)}, u32[]{:S(2)}, u32[]{:S(2)}) %collective-permute-start.4) | collective-permute-done | bytes 786464 | tf_op jit(solution)/shard_map/ppermute | solution.py:82
  108.7 2.1 constant_dynamic-update-slice_fusion.7
  110.8 1.0 constant_dynamic-update-slice_fusion.6
  111.8 0.9 constant_dynamic-update-slice_fusion.5
  112.7 0.9 constant_dynamic-update-slice_fusion.4
  113.7 2.1 constant_dynamic-update-slice_fusion.3
  115.8 0.9 constant_dynamic-update-slice_fusion.2
  116.7 1.0 constant_dynamic-update-slice_fusion.1
  117.7 0.9 constant_dynamic-update-slice_fusion
  118.6 9.5 %all-gather.4.cloned.1.call-done = bf16[2048,1408]{1,0:T(8,128)(2,1)} async-done(((bf16[256,1408]{1,0:T(8,128)(2,1)}), bf16[2048,1408]{1,0:T(8,128)(2,1)}) %all-gather.4.cloned.1.call-update) | async-done | bytes 5767184 | tf_op jit(solution)/shard_map/all_gather | solution.py:88
  128.2 9.7 %fusion.3 = f32[768,1408]{1,0:T(8,128)} fusion(bf16[2048,1408]{1,0:T(8,128)(2,1)} %all-gather.4.cloned.1.call-done, bf16[1536,2048]{1,0:T(8,128)(2,1)} %constant_dynamic-update-slice_fusion, s32[]{:T(128)S(6)} %select_n.23), kind=kOutput, calls=%fused_computation.9 | convolution fusion | flops 4429185024 | bytes 13238276 | tf_op jit(solution)/shard_map/dot_general | solution.py:86
  137.9 82.7 %all-gather.6.cloned.1.call-done = bf16[2048,1408]{1,0:T(8,128)(2,1)} async-done(((bf16[256,1408]{1,0:T(8,128)(2,1)}), bf16[2048,1408]{1,0:T(8,128)(2,1)}) %all-gather.6.cloned.1.call-update) | async-done | bytes 5767184 | tf_op jit(solution)/shard_map/all_gather | solution.py:93
  220.5 93.0 %all-gather.8.cloned.1.call-done = bf16[1408,2048]{1,0:T(8,128)(2,1)} async-done(((bf16[1408,256]{1,0:T(8,128)(2,1)}), bf16[1408,2048]{1,0:T(8,128)(2,1)}) %all-gather.8.cloned.1.call-update) | async-done | bytes 5767184 | tf_op jit(solution)/shard_map/all_gather | solution.py:99
  313.5 16.8 %convolution_convert_fusion.1 = bf16[768,2048]{1,0:T(8,128)(2,1)} fusion(bf16[1408,2048]{1,0:T(8,128)(2,1)} %all-gather.8.cloned.1.call-done, f32[768,1408]{1,0:T(8,128)} %fusion.3, bf16[2048,1408]{1,0:T(8,128)(2,1)} %all-gather.6.cloned.1.call-done, bf16[1536,2048]{1,0:T(8,128)(2,1)} %constant_dynamic-update-slice_fusion, s32[]{:T(128)S(6)} %select_n.23), kind=kOutput, calls=%fused_computation.2 | convolution fusion | flops 8866430976 | bytes 22151172 | tf_op jit(solution)/shard_map/dot_general | solution.py:97
  330.3 0.0 reduce-scatter.5.cloned.1.call-update
  330.3 36.2 %reduce-scatter.5.cloned.1.call-done = bf16[192,2048]{1,0:T(8,128)(2,1)} async-done(((bf16[768,2048]{1,0:T(8,128)(2,1)}), bf16[192,2048]{1,0:T(8,128)(2,1)}) %reduce-scatter.5.cloned.1.call-update) | async-done | bytes 786448 | tf_op jit(solution)/shard_map/reduce_scatter | solution.py:102
  366.5 0.0 copy-done.1
  366.5 2.4 fusion.11
  (13 shorter events, 0.1 us)
Async XLA Ops:
  7.4 16.0 %copy-start.5 = (f32[4]{0:T(128)S(1)}, f32[4]{0:T(128)}, u32[]{:S(2)}) copy-start(f32[4]{0:T(128)} %param.14) | copy-start | bytes 52
  7.4 64.0 %reduce-scatter.3.cloned.1.call-start = ((), (), s32[]{:S(2)}) async-start(), calls=%async_computation.2 | async-start | bytes 3932160 | tf_op jit(solution)/shard_map/reduce_scatter | solution.py:69
  8.1 13.4 %collective-permute-start.1 = (bf16[128,64]{0,1:T(8,128)(2,1)S(1)}, bf16[128,64]{0,1:T(8,128)(2,1)S(1)}, u32[]{:S(2)}, u32[]{:S(2)}) collective-permute-start(bf16[128,64]{0,1:T(8,128)(2,1)S(1)} %slice.14), channel_id=1, source_target_pairs={{0,4},{4,8},{8,12},{12,16},{16,20},{20,24},{24,28},{1,5},{5,9},{9,... | collective-permute-start | bytes 49160 | tf_op jit(solution)/shard_map/ppermute | solution.py:13
  13.7 12.1 %collective-permute-start = (bf16[128,64]{0,1:T(8,128)(2,1)S(1)}, bf16[128,64]{0,1:T(8,128)(2,1)S(1)}, u32[]{:S(2)}, u32[]{:S(2)}) collective-permute-start(bf16[128,64]{0,1:T(8,128)(2,1)S(1)} %slice.12), channel_id=1, source_target_pairs={{0,4},{4,8},{8,12},{12,16},{16,20},{20,24},{24,28},{1,5},{5,9},{9,... | collective-permute-start | bytes 49160 | tf_op jit(solution)/shard_map/ppermute | solution.py:13
  22.5 3.4 copy-start.3
  23.4 1.6 copy-start.2
  29.1 42.3 %copy-start = (bf16[192,2048]{1,0:T(8,128)(2,1)S(1)}, bf16[192,2048]{1,0:T(8,128)(2,1)}, u32[]{:S(2)}) copy-start(bf16[192,2048]{1,0:T(8,128)(2,1)} %param.10) | copy-start | bytes 2359300
  33.1 39.8 %copy-start.4 = (f32[2048]{0:T(1024)S(1)}, f32[2048]{0:T(1024)}, u32[]{:S(2)}) copy-start(f32[2048]{0:T(1024)} %param.16) | copy-start | bytes 24580
  33.1 95.0 %all-gather.4.cloned.1.call-start = ((), (), s32[]{:S(2)}) async-start(), calls=%async_computation.3 | async-start | bytes 6488064 | tf_op jit(solution)/shard_map/all_gather | solution.py:88
  33.7 186.8 %all-gather.6.cloned.1.call-start = ((), (), s32[]{:S(2)}) async-start(), calls=%async_computation.4 | async-start | bytes 6488064 | tf_op jit(solution)/shard_map/all_gather | solution.py:93
  34.3 279.2 %all-gather.8.cloned.1.call-start = ((), (), s32[]{:S(2)}) async-start(), calls=%async_computation.5 | async-start | bytes 6488064 | tf_op jit(solution)/shard_map/all_gather | solution.py:99
  34.9 331.7 %reduce-scatter.5.cloned.1.call-start = ((), (), s32[]{:S(2)}) async-start(), calls=%async_computation.6 | async-start | bytes 3932160 | tf_op jit(solution)/shard_map/reduce_scatter | solution.py:102
  74.3 11.5 %collective-permute-start.2 = (bf16[192,2048]{1,0:T(8,128)(2,1)S(1)}, bf16[192,2048]{1,0:T(8,128)(2,1)S(1)}, u32[]{:S(2)}, u32[]{:S(2)}) collective-permute-start(bf16[192,2048]{1,0:T(8,128)(2,1)S(1)} %fusion.10), channel_id=1, source_target_pairs={{0,1},{1,2},{2,3},{3,0},{4,5},{5,6},{6,7},{7,4},{8,9},{9,10},{10,1... | collective-permute-start | bytes 2359304 | tf_op jit(solution)/shard_map/ppermute | solution.py:82
  85.8 11.4 %collective-permute-start.3 = (bf16[192,2048]{1,0:T(8,128)(2,1)S(1)}, bf16[192,2048]{1,0:T(8,128)(2,1)S(1)}, u32[]{:S(2)}, u32[]{:S(2)}) collective-permute-start(bf16[192,2048]{1,0:T(8,128)(2,1)S(1)} %collective-permute-done.2), channel_id=1, source_target_pairs={{0,1},{1,2},{2,3},{3,0},{4,5},{5,6},{6,7},{7,4},{8,9},{9,10},{10,1... | collective-permute-start | bytes 2359304 | tf_op jit(solution)/shard_map/ppermute | solution.py:82
  97.2 11.5 %collective-permute-start.4 = (bf16[192,2048]{1,0:T(8,128)(2,1)S(1)}, bf16[192,2048]{1,0:T(8,128)(2,1)}, u32[]{:S(2)}, u32[]{:S(2)}) collective-permute-start(bf16[192,2048]{1,0:T(8,128)(2,1)S(1)} %collective-permute-done.3), channel_id=1, source_target_pairs={{0,1},{1,2},{2,3},{3,0},{4,5},{5,6},{6,7},{7,4},{8,9},{9,10},{10,1... | collective-permute-start | bytes 2359304 | tf_op jit(solution)/shard_map/ppermute | solution.py:82
  137.9 228.7 %copy-start.1 = (bf16[192,2048]{1,0:T(8,128)(2,1)S(1)}, bf16[192,2048]{1,0:T(8,128)(2,1)}, u32[]{:S(2)}) copy-start(bf16[192,2048]{1,0:T(8,128)(2,1)} %reduce-scatter.3.cloned.1.call-done) | copy-start | bytes 2359300
Sparse Core Ops, SparseCore 0:
  33.2 38.0 reduce-scatter.2
  330.4 36.0 reduce-scatter.4
Sparse Core Ops, SparseCore 1:
  35.8 92.3 all-gather.3
  130.2 90.2 all-gather.5
  222.4 91.0 all-gather.7
